TPU v7x, 512 devices: a 8x2x16 block of a 8x8x16 slice. The times are simulated.
512 devices in a mesh: grp: 2 (over y), ep: 32 (over z, core), tp: 8 (over x).
Axes of the slice: x: 8, y: 2, z: 16, core: 2. Of those that a mesh axis runs over, the one named last changes fastest.
The devices are a block of a 8x8x16 slice.
Arguments:
- queries: bfloat16 [8192, 1024], P(('grp', 'ep'), 'tp'), parts along dimension 0, may hold values from -6 to 6
- keys: bfloat16 [8192, 1024], P(('grp', 'ep'), 'tp'), parts along dimension 0, may hold values from -6 to 6
- values: bfloat16 [8192, 1024], P(('grp', 'ep'), 'tp'), parts along dimension 0, may hold values from -6 to 6
- lambdas: float32 [8], P('tp'), may hold values from 0.3 to 0.8
- head_gain: float32 [128], replicated, may hold values from 0.1 to 1.9
- tokens: bfloat16 [16384, 1536], P(('grp', 'ep')), parts along dimension 0, may hold values from -6 to 6
- route_ids: int32 [16384, 2], P(('grp', 'ep')), parts along dimension 0, may hold values from 0 to 31, all different within a row; in each aligned block of 256 rows (0 to 255, 256 to 511, ...) at most 32 rows name the same one
- route_weights: float32 [16384, 2], P(('grp', 'ep')), parts along dimension 0, may hold values from 0.2 to 1
- moe_gain: float32 [1536], replicated, may hold values from 0.1 to 1.9
- w_gate: bfloat16 [32, 1536, 3072], P('ep', None, 'tp'), may hold values from -0.15625 to 0.15625
- w_up: bfloat16 [32, 1536, 3072], P('ep', None, 'tp'), may hold values from -0.15625 to 0.15625
- w_down: bfloat16 [32, 3072, 1536], P('ep', 'tp'), may hold values from -0.109375 to 0.109375
Outputs:
- heads_out: bfloat16 [8192, 1024], P(('grp', 'ep'), 'tp'), parts along dimension 0
- expert_out: bfloat16 [16384, 1536], P(('grp', 'ep'), 'tp'), parts along dimension 0
There are 2 independent parts, one for each index of `grp`. A program takes and returns all parts, laid end to end along the dimension named above; an argument that names none is the same for every part. Nothing has to cross between parts.
Inputs may be any that keep to these rules, and one draw needn't show every extreme that they name: `route_ids`: each row names 2 different experts. In the 256 rows of one device no expert is named more than 32 times, and in every draw some device names some expert exactly 32 times.
All inputs are finite; a program needn't handle non-finite values.
Results may differ from a plain program's by a relative error of at most 0.015.
Values may be sent and summed in bfloat16 or wider, within the bound.
A program may use at most 64 MiB of HBM per device.

v0:
```python
import jax
import jax.numpy as jnp
from jax import lax
from jax.sharding import PartitionSpec as P


def side_by_side(arrays, axis, dim, along):
    widths = [a.shape[along] for a in arrays]
    both = jnp.concatenate(arrays, axis=along)
    filled = lax.all_gather(both, axis, axis=dim, tiled=True)
    return tuple(jnp.split(filled, [sum(widths[:k]) for k in range(1, len(widths))], axis=along))


def joined_along(parts, dim):
    parts = jnp.moveaxis(parts, 0, dim)
    lengths = parts.shape
    return parts.reshape(*lengths[:dim], lengths[dim] * lengths[dim + 1], *lengths[dim + 2 :])


def sent_to_all(shard, axis):
    copies = jnp.broadcast_to(shard, (lax.axis_size(axis), *shard.shape))
    return lax.all_to_all(copies, axis, split_axis=0, concat_axis=0, tiled=True)


def gather_directly(shard, axis, dim):
    return joined_along(sent_to_all(shard, axis), dim)


def attend(queries, keys, values, lambdas, head_gain):
    row_count = queries.shape[0]
    head_count = lambdas.shape[0]
    head_dim = queries.shape[1] // (2 * head_count)
    value_dim = values.shape[1] // head_count
    query_parts = queries.reshape(row_count, head_count, 2, head_dim)
    score_scale = head_dim ** (-0.5)
    running = jnp.full((head_count, 2, row_count), -1e30, jnp.float32)
    key_piece, value_piece = side_by_side((keys, values), "ep", 0, 1)
    count = key_piece.shape[0]
    key_parts = key_piece.reshape(count, head_count, 2, head_dim)
    value_parts = value_piece.reshape(count, head_count, value_dim)
    scores = (
        jnp.einsum("qhcd,khcd->hcqk", query_parts, key_parts, preferred_element_type=jnp.float32)
        * score_scale
    )
    newest = jnp.maximum(running, jnp.max(scores, axis=-1))
    weights_now = jnp.exp(scores - newest[..., None])
    totals = jnp.sum(weights_now, axis=-1)
    sums = jnp.einsum(
        "hcqk,khe->hcqe",
        weights_now.astype(jnp.bfloat16),
        value_parts,
        preferred_element_type=jnp.float32,
    )
    running, totals, sums = (newest, totals, sums)
    means = sums / totals[..., None]
    mixed = means[:, 0] - lambdas[:, None, None] * means[:, 1]
    scaled = mixed * lax.rsqrt(jnp.mean(mixed * mixed, axis=-1, keepdims=True) + 1e-06) * head_gain
    return (
        jnp.transpose(scaled, (1, 0, 2))
        .reshape(row_count, head_count * value_dim)
        .astype(jnp.bfloat16)
    )


def experts(tokens, route_ids, route_weights, moe_gain, w_gate, w_up, w_down):
    row_count, width = tokens.shape
    top_count = route_ids.shape[1]
    ep_size = lax.axis_size("ep")
    tp_size = lax.axis_size("tp")
    expert_count = w_gate.shape[0] * ep_size
    capacity = 2 * row_count * top_count // expert_count
    token_float = tokens.astype(jnp.float32)
    normed = (
        token_float
        * lax.rsqrt(jnp.mean(token_float * token_float, axis=1, keepdims=True) + 1e-06)
        * moe_gain
    ).astype(jnp.bfloat16)
    flat_ids = route_ids.reshape(-1)
    onehot = (flat_ids[:, None] == jnp.arange(expert_count, dtype=jnp.int32)[None, :]).astype(
        jnp.int32
    )
    earlier = jnp.cumsum(onehot, axis=0) - onehot
    position = jnp.sum(earlier * onehot, axis=1)
    slot_index = flat_ids * capacity + position
    owners = (
        jnp.full((expert_count * capacity,), row_count, jnp.int32)
        .at[slot_index]
        .set(jnp.arange(row_count * top_count, dtype=jnp.int32) // top_count)
    )
    padded = jnp.concatenate([normed, jnp.zeros((1, width), jnp.bfloat16)], axis=0)
    outgoing = padded[owners].reshape(expert_count, capacity, width)
    gate_mat = w_gate[0]
    up_mat = w_up[0]
    down_mat = w_down[0]
    slice_width = width // tp_size
    own_columns = lax.dynamic_slice_in_dim(
        outgoing, lax.axis_index("tp") * slice_width, slice_width, 2
    )
    arrived = lax.all_to_all(own_columns, "ep", split_axis=0, concat_axis=0, tiled=True)
    piece = gather_directly(arrived, "tp", 2)
    gate = jnp.einsum("scd,df->scf", piece, gate_mat, preferred_element_type=jnp.float32)
    upward = jnp.einsum("scd,df->scf", piece, up_mat, preferred_element_type=jnp.float32)
    hidden = (jax.nn.silu(gate) * upward).astype(jnp.bfloat16)
    flat_hidden = hidden.reshape(-1, hidden.shape[2])
    summed = lax.psum_scatter(
        jnp.einsum("fd,sf->ds", down_mat, flat_hidden, preferred_element_type=jnp.float32).astype(
            jnp.bfloat16
        ),
        "tp",
        scatter_dimension=0,
        tiled=True,
    )
    back = lax.all_to_all(summed, "ep", split_axis=1, concat_axis=1, tiled=True)
    picked = (
        jnp.take(back, slot_index, axis=1).astype(jnp.float32).reshape(-1, row_count, top_count)
    )
    combined = jnp.einsum("drk,rk->rd", picked, route_weights)
    return combined.astype(jnp.bfloat16)


def on_device(
    queries,
    keys,
    values,
    lambdas,
    head_gain,
    tokens,
    route_ids,
    route_weights,
    moe_gain,
    w_gate,
    w_up,
    w_down,
):
    heads_out = attend(queries, keys, values, lambdas, head_gain)
    expert_out = experts(tokens, route_ids, route_weights, moe_gain, w_gate, w_up, w_down)
    return (heads_out, expert_out)


def solution(mesh):
    in_specs = (
        P(("grp", "ep"), "tp"),
        P(("grp", "ep"), "tp"),
        P(("grp", "ep"), "tp"),
        P("tp"),
        P(),
        P(("grp", "ep"), None),
        P(("grp", "ep"), None),
        P(("grp", "ep"), None),
        P(),
        P("ep", None, "tp"),
        P("ep", None, "tp"),
        P("ep", "tp", None),
    )
    out_specs = (P(("grp", "ep"), "tp"), P(("grp", "ep"), "tp"))
    return jax.shard_map(
        on_device, mesh=mesh, in_specs=in_specs, out_specs=out_specs, check_vma=False
    )
```

profile of v0, /device:TPU:65, one launch (start us, length us, event | category | flops | bytes accessed | tf_op | source)
XLA Modules:
  0.0 339.7 jit_solution(3991329337983498056)
XLA Ops:
  8.0 0.0 copy-start
  8.0 0.0 copy-start.3
  8.1 0.9 copy.43
  9.0 0.1 eq.26
  9.2 0.1 reshape.199
  9.3 0.7 broadcast_multiply_fusion
  10.0 1.2 reduce-window.6
  11.2 0.2 slice_reduce_fusion
  11.4 0.1 copy.48
  11.6 0.1 mul.136
  11.7 0.1 fusion.23
  11.9 2.4 scatter_custom_fusion
  14.3 1.4 fusion.7
  15.7 0.0 copy-done.3
  15.7 0.9 fusion.9
  16.7 0.1 concatenate.7
  16.7 5.6 %gather_fusion = bf16[1024,1536]{1,0:T(8,128)(2,1)} fusion(bf16[257,1536]{1,0:T(8,128)(2,1)S(1)} %concatenate.7, s32[1024]{0:T(1024)S(1)} %fusion.28), kind=kCustom, calls=%fused_computation | custom fusion | bytes 6295552 | tf_op jit(solution)/shard_map/gather | solution.py:91
  22.3 1.4 constant_dynamic-slice_fusion
  23.7 78.3 %all_to_all.22 = bf16[32,32,192]{2,1,0:T(8,128)(2,1)S(1)} all-to-all(bf16[32,32,192]{2,1,0:T(8,128)(2,1)S(1)} %constant_dynamic-slice_fusion), channel_id=1, replica_groups=mesh['grp'=2,'ep'=32,'tp'=8] {'ep'}, dimensions={0} | all-to-all | bytes 786432 | tf_op jit(solution)/shard_map/all_to_all | solution.py:99
  102.0 2.5 broadcast_in_dim.36
  104.5 7.2 %all-to-all-start.1 = ((bf16[8,32,32,192]{3,2,1,0:T(8,128)(2,1)}), bf16[8,32,32,192]{3,2,1,0:T(8,128)(2,1)}, u32[]{:S(2)}, u32[]{:S(2)}) async-start(bf16[8,32,32,192]{3,2,1,0:T(8,128)(2,1)} %broadcast_in_dim.36), calls=%async_computation.1 | async-start | bytes 8388608 | tf_op jit(solution)/shard_map/all_to_all | solution.py:22
  111.7 0.1 all-gather.2.cloned.1.call-start
  111.7 0.0 copy-done.4
  111.7 0.1 copy.39
  111.8 0.0 copy-done.5
  111.9 0.1 copy.40
  112.0 0.6 pad_maximum_fusion
  112.6 0.1 all-gather.2.cloned.1.call-update
  112.7 0.2 reduce-scatter.4.cloned.1.call-start
  112.9 95.6 %all-to-all-done.1 = bf16[8,32,32,192]{3,2,1,0:T(8,128)(2,1)} async-done(((bf16[8,32,32,192]{3,2,1,0:T(8,128)(2,1)}), bf16[8,32,32,192]{3,2,1,0:T(8,128)(2,1)}, u32[]{:S(2)}, u32[]{:S(2)}) %all-to-all-start.1) | async-done | bytes 3145760 | tf_op jit(solution)/shard_map/all_to_all | solution.py:22
  208.5 8.4 %copy.49 = bf16[32,32,8,192]{3,2,1,0:T(8,128)(2,1)} copy(bf16[32,32,8,192]{3,1,0,2:T(8,128)(2,1)} %bitcast.12) | data formatting | bytes 6291456 | tf_op jit(solution)/shard_map/transpose | solution.py:15
  217.0 7.7 %reshape.202 = bf16[32,32,1536]{2,1,0:T(8,128)(2,1)} reshape(bf16[32,32,8,192]{3,2,1,0:T(8,128)(2,1)} %copy.49) | data formatting | bytes 6291456 | tf_op jit(solution)/shard_map/reshape | solution.py:17
  224.6 0.0 copy-done.10
  224.6 3.8 %fusion.12 = f32[32,32,384]{2,1,0:T(8,128)S(1)} fusion(bf16[32,32,1536]{2,1,0:T(8,128)(2,1)} %reshape.202, bf16[1,1536,384]{2,1,0:T(8,128)(2,1)S(1)} %copy-done.10), kind=kOutput, calls=%fused_computation.20 | convolution fusion | flops 1207959552 | bytes 5898240 | tf_op jit(solution)/shard_map/scd,df->scf/dot_general | solution.py:101
  228.5 0.0 copy-done.2
  228.5 0.0 copy-done.11
  228.5 1.9 multiply_convert_fusion
  230.4 0.0 copy-done
  230.4 3.5 %fusion.3 = bf16[1536,1024]{0,1:T(8,128)(2,1)} fusion(bf16[1024,384]{1,0:T(8,128)(2,1)S(1)} %bitcast.80, bf16[1,384,1536]{2,1,0:T(8,128)(2,1)S(1)} %copy-done), kind=kOutput, calls=%fused_computation.9 | convolution fusion | flops 1209532416 | bytes 5111808 | tf_op jit(solution)/shard_map/fd,sf->ds/dot_general | solution.py:106
  233.9 4.6 %copy.57 = bf16[1536,1024]{1,0:T(8,128)(2,1)} copy(bf16[1536,1024]{0,1:T(8,128)(2,1)} %fusion.3) | data formatting | bytes 6291456
  238.5 0.1 reduce-scatter.4.cloned.1.call-update
  238.6 0.1 reduce_sum.43
  238.7 0.1 copy.46
  238.8 0.4 copy-done.7
  239.2 0.2 copy.47
  239.4 0.0 copy-done.8
  239.4 0.1 copy.59
  239.6 0.1 copy.41
  240.4 0.0 all-gather.2.cloned.1.call-done
  240.4 0.0 slice-start
  240.4 35.5 %reduce-scatter.4.cloned.1.call-done = bf16[192,1024]{1,0:T(8,128)(2,1)} async-done(((bf16[1536,1024]{1,0:T(8,128)(2,1)}), bf16[192,1024]{1,0:T(8,128)(2,1)}) %reduce-scatter.4.cloned.1.call-update) | async-done | bytes 393232
  275.9 2.0 copy.58
  277.9 16.7 %all-to-all-start.2 = ((bf16[192,32,32]{0,2,1:T(8,128)(2,1)}), bf16[192,32,32]{0,2,1:T(8,128)(2,1)S(1)}, u32[]{:S(2)}, u32[]{:S(2)}) async-start(bf16[192,32,32]{0,2,1:T(8,128)(2,1)} %bitcast.20), calls=%async_computation.2 | async-start | bytes 1048576 | tf_op jit(solution)/shard_map/all_to_all | solution.py:113
  294.6 0.9 fusion.34
  295.6 0.6 fusion.1
  296.2 1.0 copy-done.1
  297.2 0.8 fusion.17
  298.1 0.1 fusion.26
  298.2 0.7 copy.50
  298.9 29.0 %all-to-all-done.2 = bf16[192,32,32]{0,2,1:T(8,128)(2,1)S(1)} async-done(((bf16[192,32,32]{0,2,1:T(8,128)(2,1)}), bf16[192,32,32]{0,2,1:T(8,128)(2,1)S(1)}, u32[]{:S(2)}, u32[]{:S(2)}) %all-to-all-start.2) | async-done | bytes 393248 | tf_op jit(solution)/shard_map/all_to_all | solution.py:113
  327.9 1.9 gather_fusion.1
  329.9 0.1 gather.11
  330.0 1.5 multiply_reduce_fusion
  331.5 0.7 copy.56
  (25 shorter events, 0.2 us)
Async XLA Ops:
  8.0 222.3 %copy-start = (bf16[1,384,1536]{2,1,0:T(8,128)(2,1)S(1)}, bf16[1,384,1536]{2,1,0:T(8,128)(2,1)}, u32[]{:S(2)}) copy-start(bf16[1,384,1536]{2,1,0:T(8,128)(2,1)} %param.23) | copy-start | bytes 3538948
  8.0 7.7 %copy-start.3 = (bf16[256,1536]{1,0:T(8,128)(2,1)S(1)}, bf16[256,1536]{1,0:T(8,128)(2,1)}, u32[]{:S(2)}) copy-start(bf16[256,1536]{1,0:T(8,128)(2,1)} %param.17) | copy-start | bytes 2359300
  104.5 7.2 %copy-start.4 = (bf16[128,128]{1,0:T(8,128)(2,1)S(1)}, bf16[128,128]{1,0:T(8,128)(2,1)}, u32[]{:S(2)}) copy-start(bf16[128,128]{1,0:T(8,128)(2,1)} %param.13) | copy-start | bytes 98308
  104.5 7.4 %copy-start.5 = (bf16[128,128]{1,0:T(8,128)(2,1)S(1)}, bf16[128,128]{1,0:T(8,128)(2,1)}, u32[]{:S(2)}) copy-start(bf16[128,128]{1,0:T(8,128)(2,1)} %param.14) | copy-start | bytes 98308
  104.5 104.0 %all-to-all-start.1 = ((bf16[8,32,32,192]{3,2,1,0:T(8,128)(2,1)}), bf16[8,32,32,192]{3,2,1,0:T(8,128)(2,1)}, u32[]{:S(2)}, u32[]{:S(2)}) async-start(bf16[8,32,32,192]{3,2,1,0:T(8,128)(2,1)} %broadcast_in_dim.36), calls=%async_computation.1 | async-start | bytes 8388608 | tf_op jit(solution)/shard_map/all_to_all | solution.py:22
  111.7 128.7 %all-gather.2.cloned.1.call-start = ((), (), s32[]{:S(2)}) async-start(), calls=%async_computation.4 | async-start | bytes 2162688 | tf_op jit(solution)/shard_map/all_gather | solution.py:10
  112.7 163.2 %reduce-scatter.4.cloned.1.call-start = ((), (), s32[]{:S(2)}) async-start(), calls=%async_computation.5 | async-start | bytes 3538944
  216.9 7.7 %copy-start.10 = (bf16[1,1536,384]{2,1,0:T(8,128)(2,1)S(1)}, bf16[1,1536,384]{2,1,0:T(8,128)(2,1)}, u32[]{:S(2)}) copy-start(bf16[1,1536,384]{2,1,0:T(8,128)(2,1)} %param.21) | copy-start | bytes 3538948
  224.6 3.8 %copy-start.2 = (bf16[32,32,1536]{2,1,0:T(8,128)(2,1)S(1)}, bf16[32,32,1536]{2,1,0:T(8,128)(2,1)}, u32[]{:S(2)}) copy-start(bf16[32,32,1536]{2,1,0:T(8,128)(2,1)} %reshape.202) | copy-start | bytes 9437188
  224.6 3.8 %copy-start.11 = (bf16[1,1536,384]{2,1,0:T(8,128)(2,1)S(1)}, bf16[1,1536,384]{2,1,0:T(8,128)(2,1)}, u32[]{:S(2)}) copy-start(bf16[1,1536,384]{2,1,0:T(8,128)(2,1)} %param.22) | copy-start | bytes 3538948
  238.5 0.7 copy-start.7
  238.5 0.9 copy-start.8
  238.5 1.0 copy-start.6
  240.4 54.2 %slice-start = ((bf16[4096,256]{0,1:T(8,128)(2,1)}), bf16[4096,128]{0,1:T(8,128)(2,1)S(1)}, s32[]{:S(2)}) async-start(bf16[4096,256]{0,1:T(8,128)(2,1)} %all-gather.2.cloned.1.call-done), calls=%async_computation.6 | async-start | bytes 2097152 | tf_op jit(solution)/shard_map/split | solution.py:11
  277.9 50.0 %all-to-all-start.2 = ((bf16[192,32,32]{0,2,1:T(8,128)(2,1)}), bf16[192,32,32]{0,2,1:T(8,128)(2,1)S(1)}, u32[]{:S(2)}, u32[]{:S(2)}) async-start(bf16[192,32,32]{0,2,1:T(8,128)(2,1)} %bitcast.20), calls=%async_computation.2 | async-start | bytes 1048576 | tf_op jit(solution)/shard_map/all_to_all | solution.py:113
  295.6 1.6 copy-start.1
  297.2 0.9 copy-start.9
Sparse Core Ops, SparseCore 0:
  115.1 68.1 all-gather.1
Sparse Core Ops, SparseCore 1:
  238.7 37.2 reduce-scatter.3
where the time goes:
time: 341 us; the launch traced here: 340 us
  waiting for transfers between devices  160 us (47%)
  blocking collectives  78.3 us (23%)
  local copies, waits for them, and re-layouts  42.3 us (12%)
  starting transfers between devices  24.2 us (7%)
  between operations  16.5 us (5%)
  matrix products  11 us (3%)
  other arithmetic  7.2 us (2%)
    all_to_all x1, waiting for transfers between devices, sent_to_all(): return lax.all_to_all(copies, axis, split_axis=0, concat_axis=0, tiled=True)  95.6 us
    all_to_all x1, blocking collectives, experts(): lax.all_to_all(own_columns, 'ep', split_axis=0, concat_axis=0, tiled=True)  78.3 us
    unnamed x3, waiting for transfers between devices  35.6 us
    all_to_all x1, waiting for transfers between devices, experts(): back = lax.all_to_all(summed, 'ep', split_axis=1, concat_axis=1, tiled=True)  29 us
    all_to_all x1, starting transfers between devices, experts(): back = lax.all_to_all(summed, 'ep', split_axis=1, concat_axis=1, tiled=True)  16.7 us
    unnamed x32, local copies, waits for them, and re-layouts  10.2 us
    transpose x1, local copies, waits for them, and re-layouts, joined_along(): parts = jnp.moveaxis(parts, 0, dim)  8.44 us
    reshape x1, local copies, waits for them, and re-layouts, joined_along(): parts.reshape(*lengths[:dim], lengths[dim] * lengths[dim + 1], *lengths[d...  7.67 us
  transfers between devices with their start and end apart: 4, of which 3 were waited for; matrix products, arithmetic and copies ran while one was open for 10% of the time, Pallas kernels for 0%

commit v1 on v0

v1 whole, which is shorter than its diff:
```python
import functools

import jax
import jax.numpy as jnp
from jax import lax
from jax.experimental import pallas as pl
from jax.experimental.pallas import tpu as pltpu
from jax.sharding import PartitionSpec as P

MESH = pl.DeviceIdType.MESH
F32 = jnp.float32
BF16 = jnp.bfloat16
RIGHT, LEFT = 0, 1


def dot(a, b):
    return jnp.dot(a, b, preferred_element_type=F32)


def dot_nt(a, b):
    return lax.dot_general(a, b, (((1,), (1,)), ((), ())), preferred_element_type=F32)


def iota(shape, dim):
    return lax.broadcasted_iota(jnp.int32, shape, dim)


def kernel(
    E,
    T,
    q_hbm,
    k_hbm,
    v_hbm,
    lam_ref,
    hgain_hbm,
    tok_hbm,
    ids_hbm,
    rw_hbm,
    mgain_hbm,
    wg_hbm,
    wu_hbm,
    wd_hbm,
    heads_ref,
    eout_ref,
    q_s,
    hgain_s,
    tok_s,
    ids_s,
    rw_s,
    mgain_s,
    wg_s,
    wu_s,
    wd_s,
    normed_s,
    out_s,
    G,
    H,
    wts_a,
    wts_p,
    wts_q,
    dsend,
    drecv,
    res,
    back,
    Kb,
    Vb,
    scores,
    loc,
    b_send,
    b_recv,
    x_send,
    x_recv,
    d_send,
    d_recv,
    e_send,
    e_recv,
    kv_send,
    kv_recv,
    sib_send,
    sib_recv,
):
    ep, tp = lax.axis_index("ep"), lax.axis_index("tp")
    nb = E // T
    Z = E // 2
    rows, width = tok_s.shape
    cap = out_s.shape[0] // nb
    lanes = 128
    tail = cap // 2

    x_to = (lax.rem(tp + 1, T), lax.rem(tp + T - 1, T))
    z_to = (lax.rem(ep + 2, E), lax.rem(ep + E - 2, E))
    sibling = ep + 1 - 2 * lax.rem(ep, 2)
    own_high = ep // T

    def hops(b):
        return (T // 2, T // 2 - 1) if b % 2 == 0 else (T // 2 - 1, T // 2)

    near_first = sorted(range(nb), key=lambda b: (min(b, nb - b), b))
    far_first = near_first[::-1]

    barrier = pltpu.get_barrier_semaphore()

    def greet(i, _):
        pl.semaphore_signal(
            barrier, inc=1, device_id={"ep": lax.rem(ep + i, E)}, device_id_type=MESH
        )
        return 0

    lax.fori_loop(1, E, greet, 0)
    for to in x_to:
        pl.semaphore_signal(barrier, inc=1, device_id={"tp": to}, device_id_type=MESH)

    local = [
        pltpu.make_async_copy(src, dst, loc.at[i])
        for i, (src, dst) in enumerate(
            (
                (ids_hbm, ids_s),
                (tok_hbm, tok_s),
                (mgain_hbm, mgain_s),
                (k_hbm, Kb.at[ep]),
                (v_hbm, Vb.at[ep]),
                (wg_hbm, wg_s),
                (wu_hbm, wu_s),
                (rw_hbm, rw_s),
                (wd_hbm, wd_s),
                (q_hbm, q_s),
                (hgain_hbm, hgain_s),
            )
        )
    ]
    c_ids, c_tok, c_mgain, c_k, c_v, c_wg, c_wu, c_rw, c_wd, c_q, c_hgain = local
    for copy in local:
        copy.start()

    c_ids.wait()
    id0, id1 = ids_s[:, 0:1], ids_s[:, 1:2]
    lower = (iota((rows, rows), 1) < iota((rows, rows), 0)).astype(F32).astype(BF16)
    first = lax.rem(tp - lax.rem(ep, T) + T, T)
    lane = iota((rows, nb * cap), 1)
    lane_slot = lax.rem(lane, cap)
    lane_block = lane // cap
    lane_expert = first + T * lax.rem(own_high + nb - lane_block, nb)
    named = (id0 == lane_expert) | (id1 == lane_expert)
    earlier = dot(lower, named.astype(F32).astype(BF16))
    chosen = jnp.where(named & (earlier == lane_slot.astype(F32)), 1.0, 0.0)
    select = jnp.transpose(chosen).astype(BF16)

    c_tok.wait()
    c_mgain.wait()
    gain = mgain_s[...]
    step_rows = 32

    def norm(i, _):
        at = pl.ds(pl.multiple_of(i * step_rows, step_rows), step_rows)
        x = tok_s[at, :].astype(F32)
        scale = lax.rsqrt(jnp.mean(x * x, axis=1, keepdims=True) + 1e-06)
        normed_s[at, :] = (x * scale * gain).astype(BF16)
        return 0

    lax.fori_loop(0, rows // step_rows, norm, 0)
    out_s[...] = dot(select, normed_s[...]).astype(BF16)

    pl.semaphore_wait(barrier, E + 1)

    def block(b):
        return pl.ds(b * cap, cap)

    def expert_of(b):
        return first + T * lax.rem(own_high + nb - b, nb)

    def dispatch(b):
        return pltpu.make_async_remote_copy(
            src_ref=out_s.at[block(b)],
            dst_ref=G.at[tp, block(b)],
            send_sem=b_send.at[b],
            recv_sem=b_recv.at[b],
            device_id={"ep": expert_of(b)},
            device_id_type=MESH,
        )

    def dispatch_here(b):
        return pltpu.make_async_copy(out_s.at[block(b)], G.at[tp, block(b)], b_recv.at[b])

    for b in far_first:

        @pl.when(expert_of(b) != ep)
        def _():
            dispatch(b).start()

        @pl.when(expert_of(b) == ep)
        def _():
            dispatch_here(b).start()

    buffers = (Kb, Vb)
    kv_hops = ((Z // 2, Z // 2 - 1), (Z // 2 - 1, Z // 2))

    def kv_copy(which, way, step):
        origin = lax.rem(ep + (2 * step if way == LEFT else 2 * E - 2 * step), E)
        return pltpu.make_async_remote_copy(
            src_ref=buffers[which].at[origin],
            dst_ref=buffers[which].at[origin],
            send_sem=kv_send.at[which, way, step],
            recv_sem=kv_recv.at[which, way, step],
            device_id={"ep": z_to[way]},
            device_id_type=MESH,
        )

    def sib_copy(which, way, step):
        origin = lax.rem(ep + (2 * step if way == LEFT else 2 * E - 2 * step), E)
        return pltpu.make_async_remote_copy(
            src_ref=buffers[which].at[origin],
            dst_ref=buffers[which].at[origin],
            send_sem=sib_send.at[which],
            recv_sem=sib_recv.at[which],
            device_id={"ep": sibling},
            device_id_type=MESH,
        )

    c_k.wait()
    c_v.wait()
    for which in (0, 1):
        kv_copy(which, RIGHT, 0).start()
        kv_copy(which, LEFT, 0).start()
        sib_copy(which, RIGHT, 0).start()

    def kv_step(s):
        for which in (0, 1):
            for way in (RIGHT, LEFT):
                kv_copy(which, way, s - 1).wait_recv()
                kv_copy(which, way, s).start()
                sib_copy(which, way, s).start()

    def kv_step_before_last():
        s = Z // 2 - 1
        for which in (0, 1):
            for way in (RIGHT, LEFT):
                kv_copy(which, way, s - 1).wait_recv()
                if s < kv_hops[which][way]:
                    kv_copy(which, way, s).start()
                sib_copy(which, way, s).start()

    def kv_step_last():
        s = Z // 2
        for which, way in ((0, RIGHT), (1, LEFT)):
            kv_copy(which, way, s - 1).wait_recv()
            sib_copy(which, way, s).start()

    c_rw.wait()
    w0, w1 = rw_s[:, 0:1], rw_s[:, 1:2]
    lane_e = iota((rows, lanes), 1)
    hit0, hit1 = id0 == lane_e, id1 == lane_e
    before = dot(lower, jnp.where(hit0 | hit1, 1.0, 0.0).astype(BF16))
    pos0 = jnp.sum(jnp.where(hit0, before, 0.0), axis=1, keepdims=True)
    pos1 = jnp.sum(jnp.where(hit1, before, 0.0), axis=1, keepdims=True)
    f0, f1 = id0.astype(F32), id1.astype(F32)
    nowhere = -1.0

    def fill(ref, slot0, slot1):
        columns = ref.shape[2]

        def tile(i, _):
            at = pl.ds(pl.multiple_of(i * lanes, lanes), lanes)
            here = (iota((rows, lanes), 1) + i * lanes).astype(F32)
            w = jnp.where(here == slot0, w0, 0.0) + jnp.where(here == slot1, w1, 0.0)
            high = w.astype(BF16)
            ref[0, :, at] = high
            ref[1, :, at] = (w - high.astype(F32)).astype(BF16)
            return 0

        lax.fori_loop(0, columns // lanes, tile, 0)

    fill(wts_a, f0 * cap + pos0, f1 * cap + pos1)
    fill(
        wts_p,
        jnp.where(pos0 < tail, f0 * tail + pos0, nowhere),
        jnp.where(pos1 < tail, f1 * tail + pos1, nowhere),
    )
    fill(
        wts_q,
        jnp.where(pos0 >= tail, f0 * tail + pos0 - tail, nowhere),
        jnp.where(pos1 >= tail, f1 * tail + pos1 - tail, nowhere),
    )

    def ring_copy(b, way, step):
        origin = lax.rem(tp + (step if way == LEFT else T - step), T)
        return pltpu.make_async_remote_copy(
            src_ref=G.at[origin, block(b)],
            dst_ref=G.at[origin, block(b)],
            send_sem=x_send.at[way, b, step],
            recv_sem=x_recv.at[way, b, step],
            device_id={"tp": x_to[way]},
            device_id_type=MESH,
        )

    def hidden_of(origin):
        x = G[origin]
        gate = dot(x, wg_s[...])
        up = dot(x, wu_s[...])
        H[origin] = (gate / (1.0 + jnp.exp(-gate)) * up).astype(BF16)

    for b in near_first:
        dispatch_here(b).wait()
        for way in (RIGHT, LEFT):
            ring_copy(b, way, 0).start()

    c_wg.wait()
    c_wu.wait()
    hidden_of(tp)

    half = T // 2
    kv_per_step = Z // T

    def gather_step(s, _):
        for b in near_first:
            for way in (RIGHT, LEFT):
                ring_copy(b, way, s - 1).wait_recv()
                if hops(b)[way] == half:
                    ring_copy(b, way, s).start()
                else:

                    @pl.when(s < half - 1)
                    def _():
                        ring_copy(b, way, s).start()

        hidden_of(lax.rem(tp + T - s, T))
        for i in range(kv_per_step):
            kv_step(kv_per_step * (s - 1) + 1 + i)
        hidden_of(lax.rem(tp + s, T))
        return 0

    lax.fori_loop(1, half, gather_step, 0)
    for s in range(kv_per_step * (half - 1) + 1, Z // 2 - 1):
        kv_step(s)
    if Z // 2 > kv_per_step * (half - 1) + 1:
        kv_step_before_last()
    for b in near_first:
        for way in (RIGHT, LEFT):
            if hops(b)[way] == half:
                ring_copy(b, way, half - 1).wait_recv()
    hidden_of(lax.rem(tp + half, T))

    c_wd.wait()

    def own_part(target, b):
        pair, odd = target // 2, lax.rem(target, 2)
        h = H[:, block(b), :].reshape(T * cap, H.shape[2])
        wa = wd_s[:, pl.ds(pl.multiple_of((3 * pair + 2 * odd) * lanes, lanes), lanes)]
        wb = wd_s[:, pl.ds(pl.multiple_of((3 * pair + 1) * lanes, lanes), lanes)]
        a = dot(h, wa).reshape(T, cap, lanes)
        m = dot(h, wb)
        m = jnp.where(odd == 1, pltpu.roll(m, lanes // 2, 1), m)
        r = pltpu.roll(m, lanes // 2, 1).reshape(T, cap, lanes)[:, tail:]
        m = m.reshape(T, cap, lanes)[:, :tail]
        low = iota((T, tail, lanes), 2) < lanes // 2
        return a, jnp.where(low, m, r)

    def partial_copy(b, way, step):
        return pltpu.make_async_remote_copy(
            src_ref=dsend.at[way, b, step],
            dst_ref=drecv.at[way, b, step],
            send_sem=d_send.at[way, b, step],
            recv_sem=d_recv.at[way, b, step],
            device_id={"tp": x_to[way]},
            device_id_type=MESH,
        )

    def pass_on(b, way, step):
        left_to_go = hops(b)[way] - step
        target = lax.rem(tp + (left_to_go if way == RIGHT else T - left_to_go), T)
        a, m = own_part(target, b)
        if step > 0:
            partial_copy(b, way, step - 1).wait_recv()
            a = a + drecv[way, b, step - 1, :, :cap].astype(F32)
            m = m + drecv[way, b, step - 1, :, cap:].astype(F32)
        dsend[way, b, step, :, :cap] = a.astype(BF16)
        dsend[way, b, step, :, cap:] = m.astype(BF16)
        partial_copy(b, way, step).start()

    def source_of(b, j):
        return lax.rem(j + T - lax.rem(ep, T), T) + T * lax.rem(b + own_high, nb)

    def send_back(b, j):
        return pltpu.make_async_remote_copy(
            src_ref=res.at[b, j],
            dst_ref=back.at[ep],
            send_sem=e_send,
            recv_sem=e_recv,
            device_id={"ep": source_of(b, j)},
            device_id_type=MESH,
        )

    def finish(b):
        a, m = own_part(tp, b)
        for way in (RIGHT, LEFT):
            last = hops(b)[way] - 1
            partial_copy(b, way, last).wait_recv()
            a = a + drecv[way, b, last, :, :cap].astype(F32)
            m = m + drecv[way, b, last, :, cap:].astype(F32)
        res[b, :, :cap] = a.astype(BF16)
        res[b, :, cap:] = m.astype(BF16)

        def send(j, _):
            @pl.when(source_of(b, j) != ep)
            def _():
                send_back(b, j).start()

            @pl.when(source_of(b, j) == ep)
            def _():
                pltpu.make_async_copy(res.at[b, j], back.at[ep], e_recv).start()

            return 0

        lax.fori_loop(0, T, send, 0)

    def attend_scores(c):
        q = q_s[...]
        mine = (iota(q.shape, 1) >= lanes // 2) == (c == 1)
        scale = (lanes // 2) ** -0.5
        q = jnp.where(mine, q.astype(F32) * scale, 0.0).astype(BF16)
        group = 4
        keys = Kb.shape[1]

        def score(i, top):
            k = Kb[pl.ds(i * group, group)].reshape(group * keys, lanes)
            s = dot_nt(q, k)
            scores[:, pl.ds(pl.multiple_of(i * group * keys, group * keys), group * keys)] = s
            for g in range(group):
                top = jnp.maximum(top, s[:, g * keys : (g + 1) * keys])
            return top

        top = lax.fori_loop(0, E // group, score, jnp.full((q.shape[0], keys), -jnp.inf, F32))
        top = jnp.max(top, axis=1, keepdims=True)

        def weigh(i, carry):
            total, sums = carry
            at = pl.ds(pl.multiple_of(i * group * keys, group * keys), group * keys)
            w = jnp.exp(scores[:, at] - top)
            for g in range(group):
                total = total + w[:, g * keys : (g + 1) * keys]
            v = Vb[pl.ds(i * group, group)].reshape(group * keys, lanes)
            return total, sums + dot(w.astype(BF16), v)

        zero = jnp.zeros((q.shape[0], keys), F32)
        total, sums = lax.fori_loop(0, E // group, weigh, (zero, jnp.zeros(q.shape, F32)))
        return sums / jnp.sum(total, axis=1, keepdims=True)

    pair_count = 2
    size = nb // pair_count
    pairs = [far_first[i * size : (i + 1) * size] for i in range(pair_count)]
    lag = half // 2
    means = {}
    for slot in range(half + 1 + lag):
        for p, members in enumerate(pairs):
            step = slot - p * lag
            if step < 0 or step > half:
                continue
            for b in members:
                for way in (RIGHT, LEFT):
                    if step < hops(b)[way]:
                        pass_on(b, way, step)
                if step == half:
                    finish(b)
        if slot == 0:
            kv_step_last()
        if slot == lag - 1:
            for which in (0, 1):
                pltpu.make_async_copy(
                    buffers[which].at[pl.ds(0, Z)],
                    buffers[which].at[pl.ds(0, Z)],
                    sib_recv.at[which],
                ).wait()
            c_q.wait()
            c_hgain.wait()
            means[0] = attend_scores(0)
        if slot == lag:
            means[1] = attend_scores(1)
            mixed = means[0] - lam_ref[0] * means[1]
            scale = lax.rsqrt(jnp.mean(mixed * mixed, axis=1, keepdims=True) + 1e-06)
            heads_ref[...] = (mixed * scale * hgain_s[...]).astype(BF16)

    pltpu.make_async_copy(back, back, e_recv).wait()
    wide = back[:, :cap, :].reshape(E * cap, lanes)
    packed = back[:, cap:, :].reshape(E * tail, lanes)
    a = dot(wts_a[0], wide) + dot(wts_a[1], wide)
    m = dot(wts_p[0], packed) + dot(wts_p[1], packed)
    n = dot(wts_q[0], packed) + dot(wts_q[1], packed)
    m = m + pltpu.roll(n, lanes // 2, 1)
    turned = pltpu.roll(a, lanes // 2, 1)
    low = iota(a.shape, 1) < lanes // 2
    odd = lax.rem(tp, 2) == 1
    eout_ref[:, :lanes] = jnp.where(odd, jnp.where(low, m, turned), a).astype(BF16)
    rest = jnp.where(odd, turned, m).astype(BF16)
    eout_ref[:, lanes:] = rest[:, : lanes // 2]

    for b in range(nb):

        @pl.when(expert_of(b) != ep)
        def _():
            dispatch(b).wait_send()

        for way in (RIGHT, LEFT):
            for step in range(hops(b)[way]):
                ring_copy(b, way, step).wait_send()
                partial_copy(b, way, step).wait_send()
    for which in (0, 1):
        for way in (RIGHT, LEFT):
            for step in range(kv_hops[which][way]):
                kv_copy(which, way, step).wait_send()
        pltpu.make_async_copy(
            buffers[which].at[pl.ds(0, Z)], buffers[which].at[pl.ds(0, Z)], sib_send.at[which]
        ).wait()
    pltpu.make_async_copy(back.at[pl.ds(0, E - 1)], back.at[pl.ds(0, E - 1)], e_send).wait()


def on_device(
    queries,
    keys,
    values,
    lambdas,
    head_gain,
    tokens,
    route_ids,
    route_weights,
    moe_gain,
    w_gate,
    w_up,
    w_down,
):
    E, T = lax.axis_size("ep"), lax.axis_size("tp")
    nb, Z = E // T, E // 2
    rows, width = tokens.shape
    cap = 2 * rows * route_ids.shape[1] // E
    q_rows, lanes = queries.shape
    units = w_gate.shape[2]
    slice_width = width // T
    block_rows = cap * slice_width // lanes
    half = T // 2
    dma = pltpu.SemaphoreType.DMA
    anywhere = pl.BlockSpec(memory_space=pl.ANY)
    scratch = [
        pltpu.VMEM((q_rows, lanes), BF16),
        pltpu.VMEM((1, lanes), F32),
        pltpu.VMEM((rows, width), BF16),
        pltpu.VMEM(route_ids.shape, jnp.int32),
        pltpu.VMEM(route_weights.shape, F32),
        pltpu.VMEM((1, width), F32),
        pltpu.VMEM((width, units), BF16),
        pltpu.VMEM((width, units), BF16),
        pltpu.VMEM((units, width), BF16),
        pltpu.VMEM((rows, width), BF16),
        pltpu.VMEM((nb * cap, width), BF16),
        pltpu.VMEM((T, nb * cap, width), BF16),
        pltpu.VMEM((T, nb * cap, units), BF16),
        pltpu.VMEM((2, rows, E * cap), BF16),
        pltpu.VMEM((2, rows, E * cap // 2), BF16),
        pltpu.VMEM((2, rows, E * cap // 2), BF16),
        pltpu.VMEM((2, nb, half, T, block_rows, lanes), BF16),
        pltpu.VMEM((2, nb, half, T, block_rows, lanes), BF16),
        pltpu.VMEM((nb, T, block_rows, lanes), BF16),
        pltpu.VMEM((E, block_rows, lanes), BF16),
        pltpu.VMEM((E, q_rows, lanes), BF16),
        pltpu.VMEM((E, q_rows, lanes), BF16),
        pltpu.VMEM((q_rows, E * q_rows), F32),
        dma((11,)),
        dma((nb,)),
        dma((nb,)),
        dma((2, nb, half)),
        dma((2, nb, half)),
        dma((2, nb, half)),
        dma((2, nb, half)),
        dma,
        dma,
        dma((2, 2, Z // 2)),
        dma((2, 2, Z // 2)),
        dma((2,)),
        dma((2,)),
    ]
    return pl.pallas_call(
        functools.partial(kernel, E, T),
        out_shape=(
            jax.ShapeDtypeStruct((q_rows, lanes), BF16),
            jax.ShapeDtypeStruct((rows, slice_width), BF16),
        ),
        in_specs=[anywhere] * 3
        + [pl.BlockSpec(memory_space=pltpu.SMEM)]
        + [anywhere] * 8,
        out_specs=(pl.BlockSpec(memory_space=pltpu.VMEM),) * 2,
        scratch_shapes=scratch,
        compiler_params=pltpu.CompilerParams(
            collective_id=0, has_side_effects=True, vmem_limit_bytes=48 * 1024 * 1024
        ),
    )(
        queries,
        keys,
        values,
        lambdas,
        head_gain.reshape(1, -1),
        tokens,
        route_ids,
        route_weights,
        moe_gain.reshape(1, -1),
        w_gate.reshape(w_gate.shape[1:]),
        w_up.reshape(w_up.shape[1:]),
        w_down.reshape(w_down.shape[1:]),
    )


def solution(mesh):
    in_specs = (
        P(("grp", "ep"), "tp"),
        P(("grp", "ep"), "tp"),
        P(("grp", "ep"), "tp"),
        P("tp"),
        P(),
        P(("grp", "ep"), None),
        P(("grp", "ep"), None),
        P(("grp", "ep"), None),
        P(),
        P("ep", None, "tp"),
        P("ep", None, "tp"),
        P("ep", "tp", None),
    )
    out_specs = (P(("grp", "ep"), "tp"), P(("grp", "ep"), "tp"))
    return jax.shard_map(
        on_device, mesh=mesh, in_specs=in_specs, out_specs=out_specs, check_vma=False
    )
```

time: 341 us -> 165 us (0.48)
  waiting for transfers between devices: 160 us -> 0 us
  Pallas kernels: 0 us -> 152 us
  blocking collectives: 78.3 us -> 0 us
  local copies, waits for them, and re-layouts: 42.3 us -> 11.6 us
  starting transfers between devices: 24.2 us -> 0 us
  between operations: 16.5 us -> 1.32 us
  matrix products: 11 us -> 0 us
  other arithmetic: 7.2 us -> 0 us
    pallas_call x0 -> x1, Pallas kernels: none -> 152 us  [on_device(): pl.pallas_call(functools.partial(kernel, E, T), out_shape=(jax.ShapeDtype...]
    all_to_all x2 -> x0, waiting for transfers between devices: 125 us -> none  [the longest x1 95.6 us: sent_to_all(): return lax.all_to_all(copies, axis, split_axis=0, concat_axis=0, tiled=True)]
    all_to_all x1 -> x0, blocking collectives: 78.3 us -> none  [experts(): lax.all_to_all(own_columns, 'ep', split_axis=0, concat_axis=0, tiled=True)]
    unnamed x3 -> x0, waiting for transfers between devices: 35.6 us -> none
    all_to_all x2 -> x0, starting transfers between devices: 23.9 us -> none  [the longest x1 16.7 us: experts(): back = lax.all_to_all(summed, 'ep', split_axis=1, concat_axis=1, tiled=True)]
    dot_general x5 -> x0, matrix products: 11 us -> none  [the longest x1 3.83 us: experts(): jnp.einsum('scd,df->scf', piece, gate_mat, preferred_element_type=jnp.flo...]
    transpose x1 -> x0, local copies, waits for them, and re-layouts: 8.44 us -> none  [joined_along(): parts = jnp.moveaxis(parts, 0, dim)]
    gather x3 -> x0, local copies, waits for them, and re-layouts: 7.69 us -> none  [the longest x1 5.61 us: experts(): outgoing = padded[owners].reshape(expert_count, capacity, width)]
  transfers between devices with their start and end apart: 4 -> 0, of which waited for: 3 -> 0; matrix products, arithmetic and copies ran while one was open for 10% -> 0% of each run, Pallas kernels for 0% -> 0%
where the time goes in v1:
time: 165 us
  Pallas kernels  152 us (92%)
  local copies, waits for them, and re-layouts  11.6 us (7%)
    pallas_call x1, Pallas kernels, on_device(): pl.pallas_call(functools.partial(kernel, E, T), out_shape=(jax.ShapeDtype...  152 us
    unnamed x19, local copies, waits for them, and re-layouts  10.1 us

profile of v1, /device:TPU:65, one launch (start us, length us, event | category | flops | bytes accessed | tf_op | source)
XLA Modules:
  0.0 164.9 jit_solution(2092588737177458339)
XLA Ops:
  1.3 0.7 reshape.20.mgain_hbm
  2.0 0.8 copy.14.ids_hbm
  2.8 0.8 copy.15.rw_hbm
  3.6 0.0 copy-start
  3.6 1.3 copy-done
  4.9 0.0 copy-start.1
  4.9 1.3 copy-done.1
  6.2 0.0 copy-start.2
  6.2 1.3 copy-done.2
  7.4 0.0 copy-start.3
  7.4 1.1 copy-done.3
  8.6 0.0 copy-start.4
  8.6 0.8 copy-done.4
  9.3 0.0 copy-start.5
  9.3 0.8 copy-done.5
  10.1 0.0 copy-start.6
  10.1 0.8 copy-done.6
  10.8 0.0 copy-start.7
  10.8 0.7 copy-done.7
  11.5 152.0 %shard_map.131 = (bf16[128,128]{1,0:T(8,128)(2,1)S(1)}, bf16[256,192]{1,0:T(8,128)(2,1)S(1)}) custom-call(bf16[128,128]{1,0:T(8,128)(2,1)S(1)} %copy-done.4, bf16[128,128]{1,0:T(8,128)(2,1)S(1)} %copy-done.5, bf16[128,128]{1,0:T(8,128)(2,1)S(1)} %copy-done.6, f32[1]{0:T(128)S(6)} %copy.18.lam_ref, f32[1,128]{1,0:T(1,128)S(1)} %bitcast.7, ...), custom_call_target="tpu_custom_call" | custom-call | tf_op jit(solution)/shard_map/pallas_call | solution.py:578
  163.5 0.7 copy.16
  164.3 0.6 copy.19
Async XLA Ops:
  3.6 1.3 copy-start
  4.9 1.3 copy-start.1
  6.2 1.3 copy-start.2
  7.4 1.1 copy-start.3
  8.6 0.8 copy-start.4
  9.3 0.8 copy-start.5
  10.1 0.8 copy-start.6
  10.8 0.7 copy-start.7

commit v2 on v1

--- a/solution.py
+++ b/solution.py
@@ -66,6 +66,7 @@
     Vb,
     scores,
     loc,
+    joined,
     b_send,
     b_recv,
     x_send,
@@ -83,9 +84,10 @@
     nb = E // T
     Z = E // 2
     rows, width = tok_s.shape
-    cap = out_s.shape[0] // nb
+    cap = out_s.shape[1]
     lanes = 128
     tail = cap // 2
+    level = ep // 2
 
     x_to = (lax.rem(tp + 1, T), lax.rem(tp + T - 1, T))
     z_to = (lax.rem(ep + 2, E), lax.rem(ep + E - 2, E))
@@ -101,12 +103,13 @@
     barrier = pltpu.get_barrier_semaphore()
 
     def greet(i, _):
-        pl.semaphore_signal(
-            barrier, inc=1, device_id={"ep": lax.rem(ep + i, E)}, device_id_type=MESH
-        )
+        @pl.when(i != ep)
+        def _():
+            pl.semaphore_signal(barrier, inc=1, device_id={"ep": i}, device_id_type=MESH)
+
         return 0
 
-    lax.fori_loop(1, E, greet, 0)
+    lax.fori_loop(2 * level, E, greet, 0)
     for to in x_to:
         pl.semaphore_signal(barrier, inc=1, device_id={"tp": to}, device_id_type=MESH)
 
@@ -132,17 +135,28 @@
     for copy in local:
         copy.start()
 
+    pl.semaphore_wait(barrier, 2 * level + 3)
+
+    def report(i, _):
+        pl.semaphore_signal(joined.at[ep], inc=1, device_id={"ep": i}, device_id_type=MESH)
+        return 0
+
+    lax.fori_loop(0, 2 * level, report, 0)
+
+    def column(row):
+        return jnp.transpose(jnp.broadcast_to(row, (lanes, rows)))
+
     c_ids.wait()
-    id0, id1 = ids_s[:, 0:1], ids_s[:, 1:2]
+    ids = ids_s[...].astype(F32)
+    id0, id1 = column(ids[0:1]), column(ids[1:2])
     lower = (iota((rows, rows), 1) < iota((rows, rows), 0)).astype(F32).astype(BF16)
     first = lax.rem(tp - lax.rem(ep, T) + T, T)
     lane = iota((rows, nb * cap), 1)
-    lane_slot = lax.rem(lane, cap)
-    lane_block = lane // cap
-    lane_expert = first + T * lax.rem(own_high + nb - lane_block, nb)
+    lane_slot = lax.rem(lane, cap).astype(F32)
+    lane_expert = (first + T * (lane // cap)).astype(F32)
     named = (id0 == lane_expert) | (id1 == lane_expert)
     earlier = dot(lower, named.astype(F32).astype(BF16))
-    chosen = jnp.where(named & (earlier == lane_slot.astype(F32)), 1.0, 0.0)
+    chosen = jnp.where(named & (earlier == lane_slot), 1.0, 0.0)
     select = jnp.transpose(chosen).astype(BF16)
 
     c_tok.wait()
@@ -158,38 +172,44 @@
         return 0
 
     lax.fori_loop(0, rows // step_rows, norm, 0)
-    out_s[...] = dot(select, normed_s[...]).astype(BF16)
-
-    pl.semaphore_wait(barrier, E + 1)
-
-    def block(b):
-        return pl.ds(b * cap, cap)
-
-    def expert_of(b):
-        return first + T * lax.rem(own_high + nb - b, nb)
-
-    def dispatch(b):
+    out_s[...] = dot(select, normed_s[...]).astype(BF16).reshape(nb, cap, width)
+
+    def dispatch(q):
         return pltpu.make_async_remote_copy(
-            src_ref=out_s.at[block(b)],
-            dst_ref=G.at[tp, block(b)],
-            send_sem=b_send.at[b],
-            recv_sem=b_recv.at[b],
-            device_id={"ep": expert_of(b)},
+            src_ref=out_s.at[q],
+            dst_ref=G.at[own_high, tp],
+            send_sem=b_send.at[q],
+            recv_sem=b_recv.at[own_high],
+            device_id={"ep": first + T * q},
             device_id_type=MESH,
         )
 
-    def dispatch_here(b):
-        return pltpu.make_async_copy(out_s.at[block(b)], G.at[tp, block(b)], b_recv.at[b])
-
-    for b in far_first:
-
-        @pl.when(expert_of(b) != ep)
+    def arrived(g):
+        return pltpu.make_async_copy(G.at[g, tp], G.at[g, tp], b_recv.at[g])
+
+    for q in range(nb):
+        expert = first + T * q
+
+        @pl.when((expert // 2 <= level) & (expert != ep))
         def _():
-            dispatch(b).start()
-
-        @pl.when(expert_of(b) == ep)
+            dispatch(q).start()
+
+        @pl.when(expert == ep)
         def _():
-            dispatch_here(b).start()
+            pltpu.make_async_copy(out_s.at[q], G.at[own_high, tp], b_recv.at[own_high]).start()
+
+    def later(z, _):
+        pl.semaphore_wait(joined.at[2 * z], 1)
+        pl.semaphore_wait(joined.at[2 * z + 1], 1)
+        q = z // (T // 2)
+
+        @pl.when((first + T * q) // 2 == z)
+        def _():
+            dispatch(q).start()
+
+        return 0
+
+    lax.fori_loop(level + 1, Z, later, 0)
 
     buffers = (Kb, Vb)
     kv_hops = ((Z // 2, Z // 2 - 1), (Z // 2 - 1, Z // 2))
@@ -245,14 +265,36 @@
             kv_copy(which, way, s - 1).wait_recv()
             sib_copy(which, way, s).start()
 
+    def ring_copy(g, way, step):
+        origin = lax.rem(tp + (step if way == LEFT else T - step), T)
+        return pltpu.make_async_remote_copy(
+            src_ref=G.at[g, origin],
+            dst_ref=G.at[g, origin],
+            send_sem=x_send.at[way, g, step],
+            recv_sem=x_recv.at[way, g, step],
+            device_id={"tp": x_to[way]},
+            device_id_type=MESH,
+        )
+
+    def hidden_of(origin):
+        x = G[:, origin].reshape(nb * cap, width)
+        gate = dot(x, wg_s[...])
+        up = dot(x, wu_s[...])
+        hidden = (gate / (1.0 + jnp.exp(-gate)) * up).astype(BF16)
+        H[:, origin] = hidden.reshape(nb, cap, hidden.shape[1])
+
+    for g in range(nb):
+        arrived(g).wait()
+        for way in (RIGHT, LEFT):
+            ring_copy(g, way, 0).start()
+
     c_rw.wait()
-    w0, w1 = rw_s[:, 0:1], rw_s[:, 1:2]
-    lane_e = iota((rows, lanes), 1)
+    w0, w1 = column(rw_s[0:1, :]), column(rw_s[1:2, :])
+    lane_e = iota((rows, lanes), 1).astype(F32)
     hit0, hit1 = id0 == lane_e, id1 == lane_e
     before = dot(lower, jnp.where(hit0 | hit1, 1.0, 0.0).astype(BF16))
     pos0 = jnp.sum(jnp.where(hit0, before, 0.0), axis=1, keepdims=True)
     pos1 = jnp.sum(jnp.where(hit1, before, 0.0), axis=1, keepdims=True)
-    f0, f1 = id0.astype(F32), id1.astype(F32)
     nowhere = -1.0
 
     def fill(ref, slot0, slot1):
@@ -269,39 +311,17 @@
 
         lax.fori_loop(0, columns // lanes, tile, 0)
 
-    fill(wts_a, f0 * cap + pos0, f1 * cap + pos1)
+    fill(wts_a, id0 * cap + pos0, id1 * cap + pos1)
     fill(
         wts_p,
-        jnp.where(pos0 < tail, f0 * tail + pos0, nowhere),
-        jnp.where(pos1 < tail, f1 * tail + pos1, nowhere),
+        jnp.where(pos0 < tail, id0 * tail + pos0, nowhere),
+        jnp.where(pos1 < tail, id1 * tail + pos1, nowhere),
     )
     fill(
         wts_q,
-        jnp.where(pos0 >= tail, f0 * tail + pos0 - tail, nowhere),
-        jnp.where(pos1 >= tail, f1 * tail + pos1 - tail, nowhere),
+        jnp.where(pos0 >= tail, id0 * tail + pos0 - tail, nowhere),
+        jnp.where(pos1 >= tail, id1 * tail + pos1 - tail, nowhere),
     )
-
-    def ring_copy(b, way, step):
-        origin = lax.rem(tp + (step if way == LEFT else T - step), T)
-        return pltpu.make_async_remote_copy(
-            src_ref=G.at[origin, block(b)],
-            dst_ref=G.at[origin, block(b)],
-            send_sem=x_send.at[way, b, step],
-            recv_sem=x_recv.at[way, b, step],
-            device_id={"tp": x_to[way]},
-            device_id_type=MESH,
-        )
-
-    def hidden_of(origin):
-        x = G[origin]
-        gate = dot(x, wg_s[...])
-        up = dot(x, wu_s[...])
-        H[origin] = (gate / (1.0 + jnp.exp(-gate)) * up).astype(BF16)
-
-    for b in near_first:
-        dispatch_here(b).wait()
-        for way in (RIGHT, LEFT):
-            ring_copy(b, way, 0).start()
 
     c_wg.wait()
     c_wu.wait()
@@ -311,7 +331,7 @@
     kv_per_step = Z // T
 
     def gather_step(s, _):
-        for b in near_first:
+        for b in range(nb):
             for way in (RIGHT, LEFT):
                 ring_copy(b, way, s - 1).wait_recv()
                 if hops(b)[way] == half:
@@ -333,7 +353,7 @@
         kv_step(s)
     if Z // 2 > kv_per_step * (half - 1) + 1:
         kv_step_before_last()
-    for b in near_first:
+    for b in range(nb):
         for way in (RIGHT, LEFT):
             if hops(b)[way] == half:
                 ring_copy(b, way, half - 1).wait_recv()
@@ -343,7 +363,7 @@
 
     def own_part(target, b):
         pair, odd = target // 2, lax.rem(target, 2)
-        h = H[:, block(b), :].reshape(T * cap, H.shape[2])
+        h = H[lax.rem(b + own_high, nb)].reshape(T * cap, H.shape[3])
         wa = wd_s[:, pl.ds(pl.multiple_of((3 * pair + 2 * odd) * lanes, lanes), lanes)]
         wb = wd_s[:, pl.ds(pl.multiple_of((3 * pair + 1) * lanes, lanes), lanes)]
         a = dot(h, wa).reshape(T, cap, lanes)
@@ -462,7 +482,7 @@
                     finish(b)
         if slot == 0:
             kv_step_last()
-        if slot == lag - 1:
+        if slot == lag:
             for which in (0, 1):
                 pltpu.make_async_copy(
                     buffers[which].at[pl.ds(0, Z)],
@@ -472,7 +492,7 @@
             c_q.wait()
             c_hgain.wait()
             means[0] = attend_scores(0)
-        if slot == lag:
+        if slot == lag + 1:
             means[1] = attend_scores(1)
             mixed = means[0] - lam_ref[0] * means[1]
             scale = lax.rsqrt(jnp.mean(mixed * mixed, axis=1, keepdims=True) + 1e-06)
@@ -494,7 +514,7 @@
 
     for b in range(nb):
 
-        @pl.when(expert_of(b) != ep)
+        @pl.when(first + T * b != ep)
         def _():
             dispatch(b).wait_send()
 
@@ -536,21 +556,21 @@
     block_rows = cap * slice_width // lanes
     half = T // 2
     dma = pltpu.SemaphoreType.DMA
-    anywhere = pl.BlockSpec(memory_space=pl.ANY)
+    anywhere = pl.BlockSpec(memory_space=pltpu.HBM)
     scratch = [
         pltpu.VMEM((q_rows, lanes), BF16),
         pltpu.VMEM((1, lanes), F32),
         pltpu.VMEM((rows, width), BF16),
-        pltpu.VMEM(route_ids.shape, jnp.int32),
-        pltpu.VMEM(route_weights.shape, F32),
+        pltpu.VMEM(route_ids.shape[::-1], jnp.int32),
+        pltpu.VMEM(route_weights.shape[::-1], F32),
         pltpu.VMEM((1, width), F32),
         pltpu.VMEM((width, units), BF16),
         pltpu.VMEM((width, units), BF16),
         pltpu.VMEM((units, width), BF16),
         pltpu.VMEM((rows, width), BF16),
-        pltpu.VMEM((nb * cap, width), BF16),
-        pltpu.VMEM((T, nb * cap, width), BF16),
-        pltpu.VMEM((T, nb * cap, units), BF16),
+        pltpu.VMEM((nb, cap, width), BF16),
+        pltpu.VMEM((nb, T, cap, width), BF16),
+        pltpu.VMEM((nb, T, cap, units), BF16),
         pltpu.VMEM((2, rows, E * cap), BF16),
         pltpu.VMEM((2, rows, E * cap // 2), BF16),
         pltpu.VMEM((2, rows, E * cap // 2), BF16),
@@ -562,6 +582,7 @@
         pltpu.VMEM((E, q_rows, lanes), BF16),
         pltpu.VMEM((q_rows, E * q_rows), F32),
         dma((11,)),
+        pltpu.SemaphoreType.REGULAR((E,)),
         dma((nb,)),
         dma((nb,)),
         dma((2, nb, half)),
@@ -587,7 +608,7 @@
         out_specs=(pl.BlockSpec(memory_space=pltpu.VMEM),) * 2,
         scratch_shapes=scratch,
         compiler_params=pltpu.CompilerParams(
-            collective_id=0, has_side_effects=True, vmem_limit_bytes=48 * 1024 * 1024
+            collective_id=0, has_side_effects=True, vmem_limit_bytes=62 * 1024 * 1024
         ),
     )(
         queries,
@@ -596,8 +617,8 @@
         lambdas,
         head_gain.reshape(1, -1),
         tokens,
-        route_ids,
-        route_weights,
+        route_ids.T,
+        route_weights.T,
         moe_gain.reshape(1, -1),
         w_gate.reshape(w_gate.shape[1:]),
         w_up.reshape(w_up.shape[1:]),

time: 165 us -> 157 us (0.952)
  local copies, waits for them, and re-layouts: 11.6 us -> 4.32 us
    unnamed x19 -> x1, local copies, waits for them, and re-layouts: 10.1 us -> 1.37 us
where the time goes in v2:
time: 157 us
  Pallas kernels  151 us (96%)
  local copies, waits for them, and re-layouts  4.32 us (3%)
    pallas_call x1, Pallas kernels, on_device(): pl.pallas_call(functools.partial(kernel, E, T), out_shape=(jax.ShapeDtype...  151 us

profile of v2, /device:TPU:65, one launch (start us, length us, event | category | flops | bytes accessed | tf_op | source)
XLA Modules:
  0.0 157.0 jit_solution(266358706024336834)
XLA Ops:
  1.3 1.3 reshape.20.mgain_hbm
  2.6 151.4 %shard_map.131 = (bf16[128,128]{1,0:T(8,128)(2,1)}, bf16[256,192]{1,0:T(8,128)(2,1)}) custom-call(bf16[128,128]{1,0:T(8,128)(2,1)} %q_hbm.1, bf16[128,128]{1,0:T(8,128)(2,1)} %k_hbm.1, bf16[128,128]{1,0:T(8,128)(2,1)} %v_hbm.1, f32[1]{0:T(128)S(6)} %copy.16.lam_ref, f32[1,128]{1,0:T(1,128)} %bitcast.11, bf16[256,1536]{1,0:T(8,128)(2,1)} %tok_hbm.1, ...), custom_call_target="tpu_custom_call" | custom-call | tf_op jit(solution)/shard_map/pallas_call | solution.py:599
  154.0 1.6 %copy.14 = bf16[256,192]{0,1:T(8,128)(2,1)} copy(bf16[256,192]{1,0:T(8,128)(2,1)} %get-tuple-element.3) | data formatting | bytes 196608 | tf_op jit(solution)/shard_map/pallas_call | solution.py:599
  155.6 1.4 copy.17

commit v3 on v2

--- a/solution.py
+++ b/solution.py
@@ -94,6 +94,12 @@
     sibling = ep + 1 - 2 * lax.rem(ep, 2)
     own_high = ep // T
 
+    def partner(high, b):
+        upper, under = high // 2, lax.rem(high, 2)
+        upper = 1 - upper if b // 2 else upper
+        under = 1 - under if b % 2 else under
+        return 2 * upper + under
+
     def hops(b):
         return (T // 2, T // 2 - 1) if b % 2 == 0 else (T // 2 - 1, T // 2)
 
@@ -161,7 +167,7 @@
 
     c_tok.wait()
     c_mgain.wait()
-    gain = mgain_s[...]
+    gain = jnp.concatenate([mgain_s[i : i + 1] for i in range(width // lanes)], axis=1)
     step_rows = 32
 
     def norm(i, _):
@@ -219,7 +225,7 @@
         return pltpu.make_async_remote_copy(
             src_ref=buffers[which].at[origin],
             dst_ref=buffers[which].at[origin],
-            send_sem=kv_send.at[which, way, step],
+            send_sem=kv_send,
             recv_sem=kv_recv.at[which, way, step],
             device_id={"ep": z_to[way]},
             device_id_type=MESH,
@@ -246,124 +252,78 @@
     def kv_step(s):
         for which in (0, 1):
             for way in (RIGHT, LEFT):
-                kv_copy(which, way, s - 1).wait_recv()
-                kv_copy(which, way, s).start()
-                sib_copy(which, way, s).start()
-
-    def kv_step_before_last():
-        s = Z // 2 - 1
-        for which in (0, 1):
-            for way in (RIGHT, LEFT):
-                kv_copy(which, way, s - 1).wait_recv()
-                if s < kv_hops[which][way]:
-                    kv_copy(which, way, s).start()
-                sib_copy(which, way, s).start()
-
-    def kv_step_last():
-        s = Z // 2
-        for which, way in ((0, RIGHT), (1, LEFT)):
-            kv_copy(which, way, s - 1).wait_recv()
-            sib_copy(which, way, s).start()
-
-    def ring_copy(g, way, step):
+                if s <= kv_hops[which][way]:
+                    kv_copy(which, way, s - 1).wait_recv()
+                    if s < kv_hops[which][way]:
+                        kv_copy(which, way, s).start()
+                    sib_copy(which, way, s).start()
+
+    half = T // 2
+    pair_count = 2
+    size = nb // pair_count
+
+    def group(k):
+        return partner(own_high, k)
+
+    def ring_copy(k, way, step):
         origin = lax.rem(tp + (step if way == LEFT else T - step), T)
         return pltpu.make_async_remote_copy(
-            src_ref=G.at[g, origin],
-            dst_ref=G.at[g, origin],
-            send_sem=x_send.at[way, g, step],
-            recv_sem=x_recv.at[way, g, step],
+            src_ref=G.at[group(k), origin],
+            dst_ref=G.at[group(k), origin],
+            send_sem=x_send,
+            recv_sem=x_recv.at[way, k, step],
             device_id={"tp": x_to[way]},
             device_id_type=MESH,
         )
 
-    def hidden_of(origin):
-        x = G[:, origin].reshape(nb * cap, width)
+    def hidden_of(p, origins):
+        places = [(group(k), o) for k in range(p * size, (p + 1) * size) for o in origins]
+        x = jnp.concatenate([G[g, o] for g, o in places], axis=0)
         gate = dot(x, wg_s[...])
         up = dot(x, wu_s[...])
         hidden = (gate / (1.0 + jnp.exp(-gate)) * up).astype(BF16)
-        H[:, origin] = hidden.reshape(nb, cap, hidden.shape[1])
-
-    for g in range(nb):
-        arrived(g).wait()
-        for way in (RIGHT, LEFT):
-            ring_copy(g, way, 0).start()
-
-    c_rw.wait()
-    w0, w1 = column(rw_s[0:1, :]), column(rw_s[1:2, :])
-    lane_e = iota((rows, lanes), 1).astype(F32)
-    hit0, hit1 = id0 == lane_e, id1 == lane_e
-    before = dot(lower, jnp.where(hit0 | hit1, 1.0, 0.0).astype(BF16))
-    pos0 = jnp.sum(jnp.where(hit0, before, 0.0), axis=1, keepdims=True)
-    pos1 = jnp.sum(jnp.where(hit1, before, 0.0), axis=1, keepdims=True)
-    nowhere = -1.0
-
-    def fill(ref, slot0, slot1):
-        columns = ref.shape[2]
-
-        def tile(i, _):
-            at = pl.ds(pl.multiple_of(i * lanes, lanes), lanes)
-            here = (iota((rows, lanes), 1) + i * lanes).astype(F32)
-            w = jnp.where(here == slot0, w0, 0.0) + jnp.where(here == slot1, w1, 0.0)
-            high = w.astype(BF16)
-            ref[0, :, at] = high
-            ref[1, :, at] = (w - high.astype(F32)).astype(BF16)
-            return 0
-
-        lax.fori_loop(0, columns // lanes, tile, 0)
-
-    fill(wts_a, id0 * cap + pos0, id1 * cap + pos1)
-    fill(
-        wts_p,
-        jnp.where(pos0 < tail, id0 * tail + pos0, nowhere),
-        jnp.where(pos1 < tail, id1 * tail + pos1, nowhere),
-    )
-    fill(
-        wts_q,
-        jnp.where(pos0 >= tail, id0 * tail + pos0 - tail, nowhere),
-        jnp.where(pos1 >= tail, id1 * tail + pos1 - tail, nowhere),
-    )
-
-    c_wg.wait()
-    c_wu.wait()
-    hidden_of(tp)
-
-    half = T // 2
-    kv_per_step = Z // T
-
-    def gather_step(s, _):
-        for b in range(nb):
-            for way in (RIGHT, LEFT):
-                ring_copy(b, way, s - 1).wait_recv()
-                if hops(b)[way] == half:
-                    ring_copy(b, way, s).start()
-                else:
-
-                    @pl.when(s < half - 1)
-                    def _():
-                        ring_copy(b, way, s).start()
-
-        hidden_of(lax.rem(tp + T - s, T))
-        for i in range(kv_per_step):
-            kv_step(kv_per_step * (s - 1) + 1 + i)
-        hidden_of(lax.rem(tp + s, T))
-        return 0
-
-    lax.fori_loop(1, half, gather_step, 0)
-    for s in range(kv_per_step * (half - 1) + 1, Z // 2 - 1):
-        kv_step(s)
-    if Z // 2 > kv_per_step * (half - 1) + 1:
-        kv_step_before_last()
-    for b in range(nb):
-        for way in (RIGHT, LEFT):
-            if hops(b)[way] == half:
-                ring_copy(b, way, half - 1).wait_recv()
-    hidden_of(lax.rem(tp + half, T))
-
-    c_wd.wait()
+        for i, (g, o) in enumerate(places):
+            H[g, o] = hidden[i * cap : (i + 1) * cap]
+
+    def combine_weights():
+        c_rw.wait()
+        w0, w1 = column(rw_s[0:1, :]), column(rw_s[1:2, :])
+        lane_e = iota((rows, lanes), 1).astype(F32)
+        hit0, hit1 = id0 == lane_e, id1 == lane_e
+        before = dot(lower, jnp.where(hit0 | hit1, 1.0, 0.0).astype(BF16))
+        pos0 = jnp.sum(jnp.where(hit0, before, 0.0), axis=1, keepdims=True)
+        pos1 = jnp.sum(jnp.where(hit1, before, 0.0), axis=1, keepdims=True)
+        nowhere = -1.0
+
+        def fill(ref, slot0, slot1):
+            columns = ref.shape[2]
+
+            def tile(i, _):
+                at = pl.ds(pl.multiple_of(i * lanes, lanes), lanes)
+                here = (iota((rows, lanes), 1) + i * lanes).astype(F32)
+                w = jnp.where(here == slot0, w0, 0.0) + jnp.where(here == slot1, w1, 0.0)
+                high = w.astype(BF16)
+                ref[0, :, at] = high
+                ref[1, :, at] = (w - high.astype(F32)).astype(BF16)
+                return 0
+
+            lax.fori_loop(0, columns // lanes, tile, 0)
+
+        fill(wts_a, id0 * cap + pos0, id1 * cap + pos1)
+        fill(
+            wts_p,
+            jnp.where(pos0 < tail, id0 * tail + pos0, nowhere),
+            jnp.where(pos1 < tail, id1 * tail + pos1, nowhere),
+        )
+        fill(
+            wts_q,
+            jnp.where(pos0 >= tail, id0 * tail + pos0 - tail, nowhere),
+            jnp.where(pos1 >= tail, id1 * tail + pos1 - tail, nowhere),
+        )
 
     def own_part(target, b):
         pair, odd = target // 2, lax.rem(target, 2)
-        h = H[lax.rem(b + own_high, nb)].reshape(T * cap, H.shape[3])
+        h = H[partner(own_high, b)].reshape(T * cap, H.shape[3])
         wa = wd_s[:, pl.ds(pl.multiple_of((3 * pair + 2 * odd) * lanes, lanes), lanes)]
         wb = wd_s[:, pl.ds(pl.multiple_of((3 * pair + 1) * lanes, lanes), lanes)]
         a = dot(h, wa).reshape(T, cap, lanes)
@@ -374,11 +334,14 @@
         low = iota((T, tail, lanes), 2) < lanes // 2
         return a, jnp.where(low, m, r)
 
+    def place(b, way, step):
+        return b * (T - 1) + (hops(b)[RIGHT] if way == LEFT else 0) + step
+
     def partial_copy(b, way, step):
         return pltpu.make_async_remote_copy(
-            src_ref=dsend.at[way, b, step],
+            src_ref=dsend.at[place(b, way, step)],
             dst_ref=drecv.at[way, b, step],
-            send_sem=d_send.at[way, b, step],
+            send_sem=d_send,
             recv_sem=d_recv.at[way, b, step],
             device_id={"tp": x_to[way]},
             device_id_type=MESH,
@@ -392,19 +355,19 @@
             partial_copy(b, way, step - 1).wait_recv()
             a = a + drecv[way, b, step - 1, :, :cap].astype(F32)
             m = m + drecv[way, b, step - 1, :, cap:].astype(F32)
-        dsend[way, b, step, :, :cap] = a.astype(BF16)
-        dsend[way, b, step, :, cap:] = m.astype(BF16)
+        dsend[place(b, way, step), :, :cap] = a.astype(BF16)
+        dsend[place(b, way, step), :, cap:] = m.astype(BF16)
         partial_copy(b, way, step).start()
 
     def source_of(b, j):
-        return lax.rem(j + T - lax.rem(ep, T), T) + T * lax.rem(b + own_high, nb)
+        return lax.rem(j + T - lax.rem(ep, T), T) + T * partner(own_high, b)
 
     def send_back(b, j):
         return pltpu.make_async_remote_copy(
             src_ref=res.at[b, j],
             dst_ref=back.at[ep],
             send_sem=e_send,
-            recv_sem=e_recv,
+            recv_sem=e_recv.at[own_high],
             device_id={"ep": source_of(b, j)},
             device_id_type=MESH,
         )
@@ -426,7 +389,7 @@
 
             @pl.when(source_of(b, j) == ep)
             def _():
-                pltpu.make_async_copy(res.at[b, j], back.at[ep], e_recv).start()
+                pltpu.make_async_copy(res.at[b, j], back.at[ep], e_recv.at[own_high]).start()
 
             return 0
 
@@ -464,46 +427,73 @@
         total, sums = lax.fori_loop(0, E // group, weigh, (zero, jnp.zeros(q.shape, F32)))
         return sums / jnp.sum(total, axis=1, keepdims=True)
 
-    pair_count = 2
-    size = nb // pair_count
-    pairs = [far_first[i * size : (i + 1) * size] for i in range(pair_count)]
-    lag = half // 2
-    means = {}
-    for slot in range(half + 1 + lag):
-        for p, members in enumerate(pairs):
-            step = slot - p * lag
+    kv_left = list(range(1, Z // 2 + 1))
+    begin = {2: half + 1, 3: half + 1, 1: half, 0: half + 2}
+    for slot in range(max(begin.values()) + half + 1):
+        for p in range(pair_count):
+            s = slot - p
+            if s < 0 or s > half:
+                continue
+            for k in range(p * size, (p + 1) * size):
+                if s == 0:
+                    arrived(group(k)).wait()
+                for way in (RIGHT, LEFT):
+                    if 0 < s <= hops(k)[way]:
+                        ring_copy(k, way, s - 1).wait_recv()
+                    if s < hops(k)[way]:
+                        ring_copy(k, way, s).start()
+            if slot == 0:
+                combine_weights()
+                c_wg.wait()
+                c_wu.wait()
+            if s == 0 or s == half:
+                hidden_of(p, [lax.rem(tp + s, T)])
+            else:
+                hidden_of(p, [lax.rem(tp + T - s, T), lax.rem(tp + s, T)])
+        if slot == half:
+            c_wd.wait()
+        for b in begin:
+            step = slot - begin[b]
             if step < 0 or step > half:
                 continue
-            for b in members:
-                for way in (RIGHT, LEFT):
-                    if step < hops(b)[way]:
-                        pass_on(b, way, step)
-                if step == half:
-                    finish(b)
-        if slot == 0:
-            kv_step_last()
-        if slot == lag:
-            for which in (0, 1):
-                pltpu.make_async_copy(
-                    buffers[which].at[pl.ds(0, Z)],
-                    buffers[which].at[pl.ds(0, Z)],
-                    sib_recv.at[which],
-                ).wait()
-            c_q.wait()
-            c_hgain.wait()
-            means[0] = attend_scores(0)
-        if slot == lag + 1:
-            means[1] = attend_scores(1)
-            mixed = means[0] - lam_ref[0] * means[1]
-            scale = lax.rsqrt(jnp.mean(mixed * mixed, axis=1, keepdims=True) + 1e-06)
-            heads_ref[...] = (mixed * scale * hgain_s[...]).astype(BF16)
-
-    pltpu.make_async_copy(back, back, e_recv).wait()
-    wide = back[:, :cap, :].reshape(E * cap, lanes)
-    packed = back[:, cap:, :].reshape(E * tail, lanes)
-    a = dot(wts_a[0], wide) + dot(wts_a[1], wide)
-    m = dot(wts_p[0], packed) + dot(wts_p[1], packed)
-    n = dot(wts_q[0], packed) + dot(wts_q[1], packed)
+            for way in (RIGHT, LEFT):
+                if step < hops(b)[way]:
+                    pass_on(b, way, step)
+            if step == half:
+                finish(b)
+        if slot > 0 and kv_left:
+            kv_step(kv_left.pop(0))
+
+    for which in (0, 1):
+        pltpu.make_async_copy(
+            buffers[which].at[pl.ds(0, Z)], buffers[which].at[pl.ds(0, Z)], sib_recv.at[which]
+        ).wait()
+    c_q.wait()
+    c_hgain.wait()
+    mean0 = attend_scores(0)
+    mean1 = attend_scores(1)
+    mixed = mean0 - lam_ref[0] * mean1
+    scale = lax.rsqrt(jnp.mean(mixed * mixed, axis=1, keepdims=True) + 1e-06)
+    heads_ref[...] = (mixed * scale * hgain_s[...]).astype(BF16)
+
+    def quarter(b, carry):
+        high = partner(own_high, b)
+        part = back.at[pl.ds(high * T, T)]
+        pltpu.make_async_copy(part, part, e_recv.at[high]).wait()
+        wide = part[:, :cap, :].reshape(T * cap, lanes)
+        packed = part[:, cap:, :].reshape(T * tail, lanes)
+        at = pl.ds(pl.multiple_of(high * T * cap, lanes), T * cap)
+        at_tail = pl.ds(pl.multiple_of(high * T * tail, lanes), T * tail)
+        a, m, n = carry
+        a = a + dot(wts_a[0, :, at], wide) + dot(wts_a[1, :, at], wide)
+        m = m + dot(wts_p[0, :, at_tail], packed) + dot(wts_p[1, :, at_tail], packed)
+        n = n + dot(wts_q[0, :, at_tail], packed) + dot(wts_q[1, :, at_tail], packed)
+        return a, m, n
+
+    carry = (jnp.zeros((rows, lanes), F32),) * 3
+    for b in far_first:
+        carry = quarter(b, carry)
+    a, m, n = carry
     m = m + pltpu.roll(n, lanes // 2, 1)
     turned = pltpu.roll(a, lanes // 2, 1)
     low = iota(a.shape, 1) < lanes // 2
@@ -518,14 +508,10 @@
         def _():
             dispatch(b).wait_send()
 
-        for way in (RIGHT, LEFT):
-            for step in range(hops(b)[way]):
-                ring_copy(b, way, step).wait_send()
-                partial_copy(b, way, step).wait_send()
+    pltpu.make_async_copy(dsend, dsend, x_send).wait()
+    pltpu.make_async_copy(dsend, dsend, d_send).wait()
+    pltpu.make_async_copy(Kb.at[pl.ds(0, E - 2)], Kb.at[pl.ds(0, E - 2)], kv_send).wait()
     for which in (0, 1):
-        for way in (RIGHT, LEFT):
-            for step in range(kv_hops[which][way]):
-                kv_copy(which, way, step).wait_send()
         pltpu.make_async_copy(
             buffers[which].at[pl.ds(0, Z)], buffers[which].at[pl.ds(0, Z)], sib_send.at[which]
         ).wait()
@@ -563,7 +549,7 @@
         pltpu.VMEM((rows, width), BF16),
         pltpu.VMEM(route_ids.shape[::-1], jnp.int32),
         pltpu.VMEM(route_weights.shape[::-1], F32),
-        pltpu.VMEM((1, width), F32),
+        pltpu.VMEM((width // lanes, lanes), F32),
         pltpu.VMEM((width, units), BF16),
         pltpu.VMEM((width, units), BF16),
         pltpu.VMEM((units, width), BF16),
@@ -574,7 +560,7 @@
         pltpu.VMEM((2, rows, E * cap), BF16),
         pltpu.VMEM((2, rows, E * cap // 2), BF16),
         pltpu.VMEM((2, rows, E * cap // 2), BF16),
-        pltpu.VMEM((2, nb, half, T, block_rows, lanes), BF16),
+        pltpu.VMEM((nb * (T - 1), T, block_rows, lanes), BF16),
         pltpu.VMEM((2, nb, half, T, block_rows, lanes), BF16),
         pltpu.VMEM((nb, T, block_rows, lanes), BF16),
         pltpu.VMEM((E, block_rows, lanes), BF16),
@@ -585,13 +571,13 @@
         pltpu.SemaphoreType.REGULAR((E,)),
         dma((nb,)),
         dma((nb,)),
-        dma((2, nb, half)),
-        dma((2, nb, half)),
-        dma((2, nb, half)),
+        dma,
         dma((2, nb, half)),
         dma,
+        dma((2, nb, half)),
         dma,
-        dma((2, 2, Z // 2)),
+        dma((nb,)),
+        dma,
         dma((2, 2, Z // 2)),
         dma((2,)),
         dma((2,)),
@@ -619,7 +605,7 @@
         tokens,
         route_ids.T,
         route_weights.T,
-        moe_gain.reshape(1, -1),
+        moe_gain.reshape(-1, lanes),
         w_gate.reshape(w_gate.shape[1:]),
         w_up.reshape(w_up.shape[1:]),
         w_down.reshape(w_down.shape[1:]),

time: 157 us -> 148 us (0.943)
  Pallas kernels: 151 us -> 143 us
    pallas_call x1, Pallas kernels: 151 us -> 143 us  [on_device(): pl.pallas_call(functools.partial(kernel, E, T), out_shape=(jax.ShapeDtype...]
where the time goes in v3:
time: 148 us; the launch traced here: 147 us
  Pallas kernels  143 us (97%)
  local copies, waits for them, and re-layouts  3.02 us (2%)
    pallas_call x1, Pallas kernels, on_device(): pl.pallas_call(functools.partial(kernel, E, T), out_shape=(jax.ShapeDtype...  143 us

profile of v3, /device:TPU:65, one launch (start us, length us, event | category | flops | bytes accessed | tf_op | source)
XLA Modules:
  0.0 147.4 jit_solution(14046880553599552551)
XLA Ops:
  1.3 143.1 %shard_map.131 = (bf16[128,128]{1,0:T(8,128)(2,1)}, bf16[256,192]{1,0:T(8,128)(2,1)}) custom-call(bf16[128,128]{1,0:T(8,128)(2,1)} %q_hbm.1, bf16[128,128]{1,0:T(8,128)(2,1)} %k_hbm.1, bf16[128,128]{1,0:T(8,128)(2,1)} %v_hbm.1, f32[1]{0:T(128)S(6)} %copy.16.lam_ref, f32[1,128]{1,0:T(1,128)} %bitcast.13, bf16[256,1536]{1,0:T(8,128)(2,1)} %tok_hbm.1, ...), custom_call_target="tpu_custom_call" | custom-call | tf_op jit(solution)/shard_map/pallas_call | solution.py:585
  144.4 1.6 %copy.14 = bf16[256,192]{0,1:T(8,128)(2,1)} copy(bf16[256,192]{1,0:T(8,128)(2,1)} %get-tuple-element.3) | data formatting | bytes 196608 | tf_op jit(solution)/shard_map/pallas_call | solution.py:585
  146.1 1.4 copy.17

commit v4 on v3

--- a/solution.py
+++ b/solution.py
@@ -193,7 +193,8 @@
     def arrived(g):
         return pltpu.make_async_copy(G.at[g, tp], G.at[g, tp], b_recv.at[g])
 
-    for q in range(nb):
+    for k in range(nb):
+        q = partner(own_high, k)
         expert = first + T * q
 
         @pl.when((expert // 2 <= level) & (expert != ep))
@@ -395,40 +396,39 @@
 
         lax.fori_loop(0, T, send, 0)
 
-    def attend_scores(c):
-        q = q_s[...]
-        mine = (iota(q.shape, 1) >= lanes // 2) == (c == 1)
-        scale = (lanes // 2) ** -0.5
-        q = jnp.where(mine, q.astype(F32) * scale, 0.0).astype(BF16)
-        group = 4
-        keys = Kb.shape[1]
-
-        def score(i, top):
-            k = Kb[pl.ds(i * group, group)].reshape(group * keys, lanes)
+    keys = Kb.shape[1]
+    span = 4
+
+    def attend():
+        q = q_s[...].astype(F32) * (lanes // 2) ** -0.5
+        first_half = iota(q.shape, 1) < lanes // 2
+        q = jnp.concatenate([jnp.where(first_half, q, 0.0), jnp.where(first_half, 0.0, q)], axis=0)
+        q = q.astype(BF16)
+        top = jnp.full((2 * keys, keys), -jnp.inf, F32)
+        for i in range(E // span):
+            k = Kb[i * span : (i + 1) * span].reshape(span * keys, lanes)
             s = dot_nt(q, k)
-            scores[:, pl.ds(pl.multiple_of(i * group * keys, group * keys), group * keys)] = s
-            for g in range(group):
+            scores[:, i * span * keys : (i + 1) * span * keys] = s
+            for g in range(span):
                 top = jnp.maximum(top, s[:, g * keys : (g + 1) * keys])
-            return top
-
-        top = lax.fori_loop(0, E // group, score, jnp.full((q.shape[0], keys), -jnp.inf, F32))
         top = jnp.max(top, axis=1, keepdims=True)
-
-        def weigh(i, carry):
-            total, sums = carry
-            at = pl.ds(pl.multiple_of(i * group * keys, group * keys), group * keys)
-            w = jnp.exp(scores[:, at] - top)
-            for g in range(group):
-                total = total + w[:, g * keys : (g + 1) * keys]
-            v = Vb[pl.ds(i * group, group)].reshape(group * keys, lanes)
-            return total, sums + dot(w.astype(BF16), v)
-
-        zero = jnp.zeros((q.shape[0], keys), F32)
-        total, sums = lax.fori_loop(0, E // group, weigh, (zero, jnp.zeros(q.shape, F32)))
-        return sums / jnp.sum(total, axis=1, keepdims=True)
+        means = []
+        for c in range(2):
+            at_rows = slice(c * keys, (c + 1) * keys)
+            high = jnp.broadcast_to(top[at_rows], (keys, span * keys))
+            total = jnp.zeros((keys, keys), F32)
+            sums = jnp.zeros((keys, lanes), F32)
+            for i in range(E // span):
+                w = jnp.exp(scores[at_rows, i * span * keys : (i + 1) * span * keys] - high)
+                for g in range(span):
+                    total = total + w[:, g * keys : (g + 1) * keys]
+                v = Vb[i * span : (i + 1) * span].reshape(span * keys, lanes)
+                sums = sums + dot(w.astype(BF16), v)
+            means.append(sums / jnp.sum(total, axis=1, keepdims=True))
+        return means
 
     kv_left = list(range(1, Z // 2 + 1))
-    begin = {2: half + 1, 3: half + 1, 1: half, 0: half + 2}
+    begin = {2: half + 1, 3: half + 1, 1: half, 0: half + 3}
     for slot in range(max(begin.values()) + half + 1):
         for p in range(pair_count):
             s = slot - p
@@ -470,8 +470,7 @@
         ).wait()
     c_q.wait()
     c_hgain.wait()
-    mean0 = attend_scores(0)
-    mean1 = attend_scores(1)
+    mean0, mean1 = attend()
     mixed = mean0 - lam_ref[0] * mean1
     scale = lax.rsqrt(jnp.mean(mixed * mixed, axis=1, keepdims=True) + 1e-06)
     heads_ref[...] = (mixed * scale * hgain_s[...]).astype(BF16)
@@ -566,7 +565,7 @@
         pltpu.VMEM((E, block_rows, lanes), BF16),
         pltpu.VMEM((E, q_rows, lanes), BF16),
         pltpu.VMEM((E, q_rows, lanes), BF16),
-        pltpu.VMEM((q_rows, E * q_rows), F32),
+        pltpu.VMEM((2 * q_rows, E * q_rows), F32),
         dma((11,)),
         pltpu.SemaphoreType.REGULAR((E,)),
         dma((nb,)),

time: 148 us -> 144 us (0.973)
  Pallas kernels: 143 us -> 139 us
    pallas_call x1, Pallas kernels: 143 us -> 139 us  [on_device(): pl.pallas_call(functools.partial(kernel, E, T), out_shape=(jax.ShapeDtype...]
where the time goes in v4:
time: 144 us; the launch traced here: 143 us
  Pallas kernels  139 us (97%)
  local copies, waits for them, and re-layouts  3.02 us (2%)
    pallas_call x1, Pallas kernels, on_device(): pl.pallas_call(functools.partial(kernel, E, T), out_shape=(jax.ShapeDtype...  139 us

profile of v4, /device:TPU:65, one launch (start us, length us, event | category | flops | bytes accessed | tf_op | source)
XLA Modules:
  0.0 143.2 jit_solution(7375782152922912382)
XLA Ops:
  1.3 138.9 %shard_map.131 = (bf16[128,128]{1,0:T(8,128)(2,1)}, bf16[256,192]{1,0:T(8,128)(2,1)}) custom-call(bf16[128,128]{1,0:T(8,128)(2,1)} %q_hbm.1, bf16[128,128]{1,0:T(8,128)(2,1)} %k_hbm.1, bf16[128,128]{1,0:T(8,128)(2,1)} %v_hbm.1, f32[1]{0:T(128)S(6)} %copy.16.lam_ref, f32[1,128]{1,0:T(1,128)} %bitcast.13, bf16[256,1536]{1,0:T(8,128)(2,1)} %tok_hbm.1, ...), custom_call_target="tpu_custom_call" | custom-call | tf_op jit(solution)/shard_map/pallas_call | solution.py:584
  140.2 1.6 %copy.14 = bf16[256,192]{0,1:T(8,128)(2,1)} copy(bf16[256,192]{1,0:T(8,128)(2,1)} %get-tuple-element.3) | data formatting | bytes 196608 | tf_op jit(solution)/shard_map/pallas_call | solution.py:584
  141.8 1.4 copy.17

commit v5 on v4

--- a/solution.py
+++ b/solution.py
@@ -144,7 +144,7 @@
     pl.semaphore_wait(barrier, 2 * level + 3)
 
     def report(i, _):
-        pl.semaphore_signal(joined.at[ep], inc=1, device_id={"ep": i}, device_id_type=MESH)
+        pl.semaphore_signal(joined.at[level], inc=1, device_id={"ep": i}, device_id_type=MESH)
         return 0
 
     lax.fori_loop(0, 2 * level, report, 0)
@@ -206,8 +206,7 @@
             pltpu.make_async_copy(out_s.at[q], G.at[own_high, tp], b_recv.at[own_high]).start()
 
     def later(z, _):
-        pl.semaphore_wait(joined.at[2 * z], 1)
-        pl.semaphore_wait(joined.at[2 * z + 1], 1)
+        pl.semaphore_wait(joined.at[z], 2)
         q = z // (T // 2)
 
         @pl.when((first + T * q) // 2 == z)
@@ -243,12 +242,13 @@
             device_id_type=MESH,
         )
 
-    c_k.wait()
-    c_v.wait()
-    for which in (0, 1):
-        kv_copy(which, RIGHT, 0).start()
-        kv_copy(which, LEFT, 0).start()
-        sib_copy(which, RIGHT, 0).start()
+    def kv_start():
+        c_k.wait()
+        c_v.wait()
+        for which in (0, 1):
+            kv_copy(which, RIGHT, 0).start()
+            kv_copy(which, LEFT, 0).start()
+            sib_copy(which, RIGHT, 0).start()
 
     def kv_step(s):
         for which in (0, 1):
@@ -348,10 +348,12 @@
             device_id_type=MESH,
         )
 
-    def pass_on(b, way, step):
+    def own_for(b, way, step):
         left_to_go = hops(b)[way] - step
         target = lax.rem(tp + (left_to_go if way == RIGHT else T - left_to_go), T)
-        a, m = own_part(target, b)
+        return own_part(target, b)
+
+    def pass_on(b, way, step, a, m):
         if step > 0:
             partial_copy(b, way, step - 1).wait_recv()
             a = a + drecv[way, b, step - 1, :, :cap].astype(F32)
@@ -373,8 +375,7 @@
             device_id_type=MESH,
         )
 
-    def finish(b):
-        a, m = own_part(tp, b)
+    def finish(b, a, m):
         for way in (RIGHT, LEFT):
             last = hops(b)[way] - 1
             partial_copy(b, way, last).wait_recv()
@@ -443,6 +444,7 @@
                     if s < hops(k)[way]:
                         ring_copy(k, way, s).start()
             if slot == 0:
+                kv_start()
                 combine_weights()
                 c_wg.wait()
                 c_wu.wait()
@@ -452,15 +454,19 @@
                 hidden_of(p, [lax.rem(tp + T - s, T), lax.rem(tp + s, T)])
         if slot == half:
             c_wd.wait()
+        work = []
         for b in begin:
             step = slot - begin[b]
-            if step < 0 or step > half:
-                continue
-            for way in (RIGHT, LEFT):
-                if step < hops(b)[way]:
-                    pass_on(b, way, step)
+            if 0 <= step < half:
+                ways = [way for way in (RIGHT, LEFT) if step < hops(b)[way]]
+                work.extend((b, way, step, *own_for(b, way, step)) for way in ways)
             if step == half:
-                finish(b)
+                work.append((b, None, step, *own_part(tp, b)))
+        for b, way, step, a, m in work:
+            if way is None:
+                finish(b, a, m)
+            else:
+                pass_on(b, way, step, a, m)
         if slot > 0 and kv_left:
             kv_step(kv_left.pop(0))
 
@@ -567,7 +573,7 @@
         pltpu.VMEM((E, q_rows, lanes), BF16),
         pltpu.VMEM((2 * q_rows, E * q_rows), F32),
         dma((11,)),
-        pltpu.SemaphoreType.REGULAR((E,)),
+        pltpu.SemaphoreType.REGULAR((Z,)),
         dma((nb,)),
         dma((nb,)),
         dma,

time: 144 us -> 145 us (level)
  no operation moved by 1% of the time
where the time goes in v5:
time: 145 us; the launch traced here: 143 us
  Pallas kernels  139 us (96%)
  local copies, waits for them, and re-layouts  3.02 us (2%)
    pallas_call x1, Pallas kernels, on_device(): pl.pallas_call(functools.partial(kernel, E, T), out_shape=(jax.ShapeDtype...  139 us

profile of v5, /device:TPU:65, one launch (start us, length us, event | category | flops | bytes accessed | tf_op | source)
XLA Modules:
  0.0 143.5 jit_solution(6252878038052153238)
XLA Ops:
  1.3 139.2 %shard_map.131 = (bf16[128,128]{1,0:T(8,128)(2,1)}, bf16[256,192]{1,0:T(8,128)(2,1)}) custom-call(bf16[128,128]{1,0:T(8,128)(2,1)} %q_hbm.1, bf16[128,128]{1,0:T(8,128)(2,1)} %k_hbm.1, bf16[128,128]{1,0:T(8,128)(2,1)} %v_hbm.1, f32[1]{0:T(128)S(6)} %copy.16.lam_ref, f32[1,128]{1,0:T(1,128)} %bitcast.13, bf16[256,1536]{1,0:T(8,128)(2,1)} %tok_hbm.1, ...), custom_call_target="tpu_custom_call" | custom-call | tf_op jit(solution)/shard_map/pallas_call | solution.py:590
  140.5 1.6 %copy.14 = bf16[256,192]{0,1:T(8,128)(2,1)} copy(bf16[256,192]{1,0:T(8,128)(2,1)} %get-tuple-element.3) | data formatting | bytes 196608 | tf_op jit(solution)/shard_map/pallas_call | solution.py:590
  142.1 1.4 copy.17
